TPU v7x, 256 devices: a whole 4x4x8 slice. The times are simulated.
256 devices in a mesh: fs: 16 (over y, x), tp: 16 (over z, core).
Axes of the slice: x: 4, y: 4, z: 8, core: 2. Of those that a mesh axis runs over, the one named last changes fastest.
Arguments:
- normed: bfloat16 [16384, 4096], P('fs'), may hold values from -6 to 6
- query_cotangent: bfloat16 [16384, 4096], P('fs', 'tp'), may hold values from -0.059814453 to 0.059814453
- attended: bfloat16 [16384, 4096], P('fs', 'tp'), may hold values from -6 to 6
- output_cotangent: bfloat16 [16384, 4096], P('fs'), may hold values from -0.059814453 to 0.059814453
- query_basis: bfloat16 [4096, 128], replicated, may hold values from -0.09375 to 0.09375
- output_basis: bfloat16 [4096, 128], replicated, may hold values from -0.09375 to 0.09375
- query_master: float32 [4096, 4096], P('fs', 'tp'), may hold values from -0.6 to 0.6
- output_master: float32 [4096, 4096], P('fs', 'tp'), may hold values from -0.6 to 0.6
- query_first: float32 [128, 4096], P('fs', 'tp'), may hold values from -3 to 3
- query_second: float32 [128, 4096], P('fs', 'tp'), may hold values from 0.1 to 1
- output_first: float32 [128, 4096], P('fs', 'tp'), may hold values from -3 to 3
- output_second: float32 [128, 4096], P('fs', 'tp'), may hold values from 0.1 to 1
Outputs:
- query_first_new: float32 [128, 4096], P('fs', 'tp')
- query_second_new: float32 [128, 4096], P('fs', 'tp')
- query_step: float32 [4096, 4096], P('fs', 'tp')
- query_new: float32 [4096, 4096], P('fs', 'tp')
- query_copy: bfloat16 [4096, 4096], P(None, 'tp')
- output_first_new: float32 [128, 4096], P('fs', 'tp')
- output_second_new: float32 [128, 4096], P('fs', 'tp')
- output_step: float32 [4096, 4096], P('fs', 'tp')
- output_new: float32 [4096, 4096], P('fs', 'tp')
- output_copy: bfloat16 [4096, 4096], P(None, 'tp')
All inputs are finite; a program needn't handle non-finite values.
Results may differ from a plain program's by a relative error of at most 0.0065.
Values may be sent and summed in bfloat16 or wider, within the bound.
A program may use at most 128 MiB of HBM per device.

v0:
```python
import jax
import jax.numpy as jnp
from jax import lax
from jax.sharding import PartitionSpec as P

FIRST_DECAY = 0.7
SECOND_DECAY = 0.8
SECOND_FLOOR = 0.05
SCALE_FLOOR = 0.01
LEARN_RATE = 0.05
CONTRACT = (((0,), (0,)), ((), ()))


def cut_along(value, dim, devices):
    before, after = (value.shape[:dim], value.shape[dim + 1 :])
    return jnp.moveaxis(value.reshape(*before, devices, -1, *after), dim, 0)


def sum_at_owner(value, axis, dim):
    devices = lax.axis_size(axis)
    pieces = lax.all_to_all(cut_along(value, dim, devices), axis, 0, 0, tiled=True)
    return jnp.sum(pieces, axis=0)


def sent_together(arrays, axis, dim, along):
    widths = [a.shape[along] for a in arrays]
    both = jnp.concatenate(arrays, axis=along)
    result = sum_at_owner(both, axis, dim)
    return tuple(jnp.split(result, [sum(widths[:k]) for k in range(1, len(widths))], axis=along))


def side_by_side(arrays, axis, dim, along):
    ends, at = ([], 0)
    for a in arrays[:-1]:
        at += a.shape[along]
        ends.append(at)
    both = jnp.concatenate(arrays, axis=along)
    return tuple(jnp.split(lax.all_gather(both, axis, axis=dim, tiled=True), ends, axis=along))


def copy_for_each(value, axis):
    copies = jnp.broadcast_to(value, (lax.axis_size(axis), *value.shape))
    return lax.all_to_all(copies, axis, split_axis=0, concat_axis=0, tiled=True)


def taken_together(value, axis):
    everything = copy_for_each(value, axis)
    return jnp.sum(everything, axis=0)


def together(arrays, axis):
    ends = [0]
    for a in arrays:
        ends.append(ends[-1] + a.size)
    running = taken_together(jnp.concatenate([a.ravel() for a in arrays]), axis)
    return tuple((running[b:e].reshape(a.shape) for a, b, e in zip(arrays, ends, ends[1:])))


def moments(lowered, first, second):
    first_new = FIRST_DECAY * first + (1.0 - FIRST_DECAY) * lowered
    second_new = SECOND_DECAY * second + (1.0 - SECOND_DECAY) * lowered * lowered
    return (first_new, second_new, first_new / jnp.sqrt(second_new + SECOND_FLOOR))


def quadratic(basis, ratios):
    gram = lax.dot_general(basis, basis, CONTRACT, preferred_element_type=jnp.float32)
    return jnp.sum(ratios * jnp.dot(gram, ratios, precision=lax.Precision.HIGHEST))


def split_project(basis, gradient):
    high_part = gradient.astype(jnp.bfloat16)
    remain = gradient - high_part.astype(jnp.float32)
    middle_part = remain.astype(jnp.bfloat16)
    low_part = (remain - middle_part.astype(jnp.float32)).astype(jnp.bfloat16)
    high_term = lax.dot_general(basis, high_part, CONTRACT, preferred_element_type=jnp.float32)
    middle_term = lax.dot_general(basis, middle_part, CONTRACT, preferred_element_type=jnp.float32)
    low_term = lax.dot_general(basis, low_part, CONTRACT, preferred_element_type=jnp.float32)
    return high_term + (middle_term + low_term)


def body(
    normed,
    query_cotangent,
    attended,
    output_cotangent,
    query_basis,
    output_basis,
    query_master,
    output_master,
    query_first,
    query_second,
    output_first,
    output_second,
):
    row_count = query_master.shape[0]
    columns = query_master.shape[1]
    row_start = lax.axis_index("fs") * row_count
    query_wide = query_basis.astype(jnp.float32)
    output_wide = output_basis.astype(jnp.float32)
    query_rows = lax.dynamic_slice_in_dim(query_wide, row_start, row_count, 0)
    output_rows = lax.dynamic_slice_in_dim(output_wide, row_start, row_count, 0)
    grad_query = lax.dot_general(
        normed, query_cotangent, CONTRACT, preferred_element_type=jnp.float32
    )
    grad_output = lax.dot_general(
        output_cotangent, attended, CONTRACT, preferred_element_type=jnp.float32
    )
    query_term = split_project(query_basis, grad_query)
    output_term = split_project(output_basis, grad_output)
    query_low, output_low = sent_together((query_term, output_term), "fs", 0, 1)
    query_first_new, query_second_new, query_ratio = moments(query_low, query_first, query_second)
    output_first_new, output_second_new, output_ratio = moments(
        output_low, output_first, output_second
    )
    query_full, output_full = side_by_side((query_ratio, output_ratio), "fs", 0, 1)
    query_update = jnp.dot(query_rows, query_full, precision=lax.Precision.HIGHEST)
    output_update = jnp.dot(output_rows, output_full, precision=lax.Precision.HIGHEST)
    query_total, output_total = together(
        (quadratic(query_basis, query_full), quadratic(output_basis, output_full)), "tp"
    )
    entries = normed.shape[1] * columns * lax.axis_size("tp")
    query_step = query_update * lax.rsqrt(query_total / entries + SCALE_FLOOR)
    output_step = output_update * lax.rsqrt(output_total / entries + SCALE_FLOOR)
    query_new = query_master - LEARN_RATE * query_step
    output_new = output_master - LEARN_RATE * output_step
    query_copy, output_copy = side_by_side(
        (query_new.astype(jnp.bfloat16), output_new.astype(jnp.bfloat16)), "fs", 0, 1
    )
    return (
        query_first_new,
        query_second_new,
        query_step,
        query_new,
        query_copy,
        output_first_new,
        output_second_new,
        output_step,
        output_new,
        output_copy,
    )


def solution(mesh):
    in_specs = (
        P("fs", None),
        P("fs", "tp"),
        P("fs", "tp"),
        P("fs", None),
        P(),
        P(),
        P("fs", "tp"),
        P("fs", "tp"),
        P("fs", "tp"),
        P("fs", "tp"),
        P("fs", "tp"),
        P("fs", "tp"),
    )
    out_specs = (
        P("fs", "tp"),
        P("fs", "tp"),
        P("fs", "tp"),
        P("fs", "tp"),
        P(None, "tp"),
        P("fs", "tp"),
        P("fs", "tp"),
        P("fs", "tp"),
        P("fs", "tp"),
        P(None, "tp"),
    )
    return jax.shard_map(body, mesh=mesh, in_specs=in_specs, out_specs=out_specs, check_vma=False)
```

profile of v0, /device:TPU:1, one launch (start us, length us, event | category | flops | bytes accessed | tf_op | source)
XLA Modules:
  0.0 158.3 jit_solution(1471813160837848556)
XLA Ops:
  7.2 0.0 copy-start
  7.2 0.0 copy-start.1
  7.2 6.1 %fusion.48 = f32[4096,256]{1,0:T(8,128)S(1)} fusion(bf16[1024,4096]{1,0:T(8,128)(2,1)} %param.12, bf16[1024,256]{1,0:T(8,128)(2,1)} %param.13), kind=kOutput, calls=%fused_computation.52 | convolution fusion | flops 2147483648 | bytes 13107200 | tf_op jit(solution)/shard_map/dot_general | solution.py:102
  13.4 0.0 copy-done.1
  13.4 0.0 copy-start.8
  13.4 0.0 copy-start.9
  13.4 0.8 fusion.10
  14.2 0.8 fusion.1
  15.0 1.8 %copy-done.8 = bf16[1024,4096]{1,0:T(8,128)(2,1)S(1)} copy-done((bf16[1024,4096]{1,0:T(8,128)(2,1)S(1)}, bf16[1024,4096]{1,0:T(8,128)(2,1)}, u32[]{:S(2)}) %copy-start.8) | copy-done | bytes 8388632
  16.7 0.0 copy-done.9
  16.8 2.6 %fusion.49 = f32[4096,256]{1,0:T(8,128)S(1)} fusion(bf16[1024,4096]{1,0:T(8,128)(2,1)S(1)} %copy-done.8, bf16[1024,256]{1,0:T(8,128)(2,1)S(1)} %copy-done.9), kind=kOutput, calls=%fused_computation.53 | convolution fusion | flops 2147483648 | bytes 13107200 | tf_op jit(solution)/shard_map/dot_general | solution.py:105
  19.4 0.0 copy-done
  19.4 0.8 fusion.11
  20.2 0.8 fusion.6
  21.0 0.8 fusion.27
  21.8 0.8 fusion.18
  22.6 0.0 copy-start.4
  22.6 0.0 copy-start.5
  22.6 0.0 copy-start.6
  22.6 0.0 copy-start.7
  22.7 0.0 copy-start.2
  22.7 0.0 copy-start.3
  22.7 0.8 copy.48
  23.5 7.6 %all-to-all-start = ((f32[16,8,512]{2,1,0:T(8,128)}), f32[16,8,512]{2,1,0:T(8,128)S(1)}, u32[]{:S(2)}, u32[]{:S(2)}) async-start(f32[16,8,512]{2,1,0:T(8,128)} %bitcast.2), calls=%async_computation | async-start | bytes 524288 | tf_op jit(solution)/shard_map/all_to_all | solution.py:21
  31.1 0.5 fusion.50
  31.6 0.5 fusion.51
  32.1 6.6 %all-to-all-done = f32[16,8,512]{2,1,0:T(8,128)S(1)} async-done(((f32[16,8,512]{2,1,0:T(8,128)}), f32[16,8,512]{2,1,0:T(8,128)S(1)}, u32[]{:S(2)}, u32[]{:S(2)}) %all-to-all-start) | async-done | bytes 262176 | tf_op jit(solution)/shard_map/all_to_all | solution.py:21
  38.7 0.0 copy-done.4
  38.7 0.0 copy-done.5
  38.7 0.0 copy-done.6
  38.7 0.0 copy-done.7
  38.7 0.6 rsqrt_multiply_fusion
  39.4 16.4 %all_gather.6 = f32[128,512]{1,0:T(8,128)S(1)} all-gather(f32[8,512]{1,0:T(8,128)S(1)} %pad_maximum_fusion.2), channel_id=1, replica_groups=mesh['fs'=16,'tp'=16] {'fs'}, dimensions={0}, use_global_device_ids=true | all-gather | bytes 278528 | tf_op jit(solution)/shard_map/all_gather | solution.py:38
  55.8 0.9 fusion.30
  56.6 0.9 fusion.31
  57.5 1.4 pad_maximum_fusion.3
  58.9 0.6 broadcast_in_dim.3
  59.5 15.9 %all-to-all-start.1 = ((f32[16,1,2]{2,1,0:T(1,128)}), f32[16,1,2]{2,1,0:T(1,128)S(1)}, u32[]{:S(2)}, u32[]{:S(2)}) async-start(f32[16,1,2]{2,1,0:T(1,128)} %broadcast_in_dim.3), calls=%async_computation.1 | async-start | bytes 16384 | tf_op jit(solution)/shard_map/all_to_all | solution.py:43
  75.4 0.0 all-gather.2.cloned.1.call-start
  75.4 0.0 copy-done.2
  75.4 0.1 copy.50
  75.5 0.0 copy-done.3
  75.6 0.1 copy.51
  75.7 6.6 %all-to-all-done.1 = f32[16,1,2]{2,1,0:T(1,128)S(1)} async-done(((f32[16,1,2]{2,1,0:T(1,128)}), f32[16,1,2]{2,1,0:T(1,128)S(1)}, u32[]{:S(2)}, u32[]{:S(2)}) %all-to-all-start.1) | async-done | bytes 160 | tf_op jit(solution)/shard_map/all_to_all | solution.py:43
  82.4 0.6 fusion.47
  84.3 0.3 fusion.43
  84.7 1.0 fusion.42
  85.7 0.7 pad_maximum_fusion.1
  86.4 0.0 all-gather.2.cloned.1.call-update
  86.4 1.8 %copy.53 = f32[256,256]{1,0:T(8,128)} copy(f32[256,256]{0,1:T(8,128)} %get-tuple-element.51) | data formatting | bytes 524288
  88.2 0.8 copy.52
  89.0 0.8 copy.56
  89.9 0.8 copy.55
  90.7 50.3 %all-gather.2.cloned.1.call-done = bf16[4096,512]{0,1:T(8,128)(2,1)} async-done(((bf16[256,512]{0,1:T(8,128)(2,1)}), bf16[4096,512]{0,1:T(8,128)(2,1)}) %all-gather.2.cloned.1.call-update) | async-done | bytes 4194320 | tf_op jit(solution)/shard_map/all_gather | solution.py:38
  141.0 3.9 %fusion.46 = (bf16[4096,256]{0,1:T(8,128)(2,1)}, bf16[4096,256]{0,1:T(8,128)(2,1)S(1)}) fusion(bf16[4096,512]{0,1:T(8,128)(2,1)} %all-gather.2.cloned.1.call-done), kind=kLoop, calls=%fused_computation.50 | loop fusion | bytes 8388608 | tf_op jit(solution)/shard_map/split | solution.py:38
  145.0 4.1 %copy.57 = bf16[4096,256]{1,0:T(8,128)(2,1)} copy(bf16[4096,256]{0,1:T(8,128)(2,1)} %get-tuple-element.60) | data formatting | bytes 4194304
  149.0 2.4 %copy.54 = bf16[4096,256]{1,0:T(8,128)(2,1)} copy(bf16[4096,256]{0,1:T(8,128)(2,1)S(1)} %get-tuple-element.61) | data formatting | bytes 4194304
  (4 shorter events, 0.1 us)
Async XLA Ops:
  7.2 12.2 %copy-start = (bf16[4096,128]{1,0:T(8,128)(2,1)S(1)}, bf16[4096,128]{1,0:T(8,128)(2,1)}, u32[]{:S(2)}) copy-start(bf16[4096,128]{1,0:T(8,128)(2,1)} %param.17) | copy-start | bytes 3145732
  7.2 6.2 %copy-start.1 = (bf16[4096,128]{1,0:T(8,128)(2,1)S(1)}, bf16[4096,128]{1,0:T(8,128)(2,1)}, u32[]{:S(2)}) copy-start(bf16[4096,128]{1,0:T(8,128)(2,1)} %param.16) | copy-start | bytes 3145732
  13.4 3.4 %copy-start.8 = (bf16[1024,4096]{1,0:T(8,128)(2,1)S(1)}, bf16[1024,4096]{1,0:T(8,128)(2,1)}, u32[]{:S(2)}) copy-start(bf16[1024,4096]{1,0:T(8,128)(2,1)} %param.15) | copy-start | bytes 25165828
  13.4 3.4 %copy-start.9 = (bf16[1024,256]{1,0:T(8,128)(2,1)S(1)}, bf16[1024,256]{1,0:T(8,128)(2,1)}, u32[]{:S(2)}) copy-start(bf16[1024,256]{1,0:T(8,128)(2,1)} %param.14) | copy-start | bytes 1572868
  22.6 16.1 %copy-start.4 = (f32[8,256]{1,0:T(8,128)S(1)}, f32[8,256]{1,0:T(8,128)}, u32[]{:S(2)}) copy-start(f32[8,256]{1,0:T(8,128)} %param.23) | copy-start | bytes 24580
  22.6 16.1 %copy-start.5 = (f32[8,256]{1,0:T(8,128)S(1)}, f32[8,256]{1,0:T(8,128)}, u32[]{:S(2)}) copy-start(f32[8,256]{1,0:T(8,128)} %param.22) | copy-start | bytes 24580
  22.6 16.1 %copy-start.6 = (f32[8,256]{1,0:T(8,128)S(1)}, f32[8,256]{1,0:T(8,128)}, u32[]{:S(2)}) copy-start(f32[8,256]{1,0:T(8,128)} %param.21) | copy-start | bytes 24580
  22.6 16.1 %copy-start.7 = (f32[8,256]{1,0:T(8,128)S(1)}, f32[8,256]{1,0:T(8,128)}, u32[]{:S(2)}) copy-start(f32[8,256]{1,0:T(8,128)} %param.20) | copy-start | bytes 24580
  22.7 52.8 %copy-start.2 = (f32[256,256]{1,0:T(8,128)S(1)}, f32[256,256]{1,0:T(8,128)}, u32[]{:S(2)}) copy-start(f32[256,256]{1,0:T(8,128)} %param.18) | copy-start | bytes 786436
  22.7 52.9 %copy-start.3 = (f32[256,256]{1,0:T(8,128)S(1)}, f32[256,256]{1,0:T(8,128)}, u32[]{:S(2)}) copy-start(f32[256,256]{1,0:T(8,128)} %param.19) | copy-start | bytes 786436
  23.5 15.1 %all-to-all-start = ((f32[16,8,512]{2,1,0:T(8,128)}), f32[16,8,512]{2,1,0:T(8,128)S(1)}, u32[]{:S(2)}, u32[]{:S(2)}) async-start(f32[16,8,512]{2,1,0:T(8,128)} %bitcast.2), calls=%async_computation | async-start | bytes 524288 | tf_op jit(solution)/shard_map/all_to_all | solution.py:21
  59.5 22.9 %all-to-all-start.1 = ((f32[16,1,2]{2,1,0:T(1,128)}), f32[16,1,2]{2,1,0:T(1,128)S(1)}, u32[]{:S(2)}, u32[]{:S(2)}) async-start(f32[16,1,2]{2,1,0:T(1,128)} %broadcast_in_dim.3), calls=%async_computation.1 | async-start | bytes 16384 | tf_op jit(solution)/shard_map/all_to_all | solution.py:43
  75.4 65.7 %all-gather.2.cloned.1.call-start = ((), (), s32[]{:S(2)}) async-start(), calls=%async_computation.2 | async-start | bytes 4456448 | tf_op jit(solution)/shard_map/all_gather | solution.py:38
Sparse Core Ops, SparseCore 0:
  86.5 54.4 all-gather.1
where the time goes:
time: 159 us; the launch traced here: 158 us
  waiting for transfers between devices  63.5 us (40%)
  starting transfers between devices  23.5 us (15%)
  local copies, waits for them, and re-layouts  18.9 us (12%)
  matrix products  17.5 us (11%)
  blocking collectives  16.4 us (10%)
  between operations  15.7 us (10%)
  other arithmetic  2.78 us (2%)
    all_gather x1, waiting for transfers between devices, side_by_side(): lax.all_gather(both, axis, axis=dim, tiled=True)  50.3 us
    all_gather x1, blocking collectives, side_by_side(): lax.all_gather(both, axis, axis=dim, tiled=True)  16.4 us
    all_to_all x1, starting transfers between devices, copy_for_each(): return lax.all_to_all(copies, axis, split_axis=0, concat_axis=0, tiled=True)  15.9 us
    unnamed x28, local copies, waits for them, and re-layouts  12.9 us
    all_to_all x1, starting transfers between devices, sum_at_owner(): lax.all_to_all(cut_along(value, dim, devices), axis, 0, 0, tiled=True)  7.57 us
    all_to_all x1, waiting for transfers between devices, copy_for_each(): return lax.all_to_all(copies, axis, split_axis=0, concat_axis=0, tiled=True)  6.63 us
    all_to_all x1, waiting for transfers between devices, sum_at_owner(): lax.all_to_all(cut_along(value, dim, devices), axis, 0, 0, tiled=True)  6.58 us
    dot_general x1, matrix products, body(): lax.dot_general(normed, query_cotangent, CONTRACT, preferred_element_type...  6.14 us
  transfers between devices with their start and end apart: 3, of which 3 were waited for; matrix products, arithmetic and copies ran while one was open for 3% of the time, Pallas kernels for 0%

commit v1 on v0

v1 whole, which is shorter than its diff:
```python
import jax
import jax.numpy as jnp
from jax import lax
from jax.experimental import pallas as pl
from jax.experimental.pallas import tpu as pltpu
from jax.sharding import PartitionSpec as P

FIRST_DECAY = 0.7
SECOND_DECAY = 0.8
SECOND_FLOOR = 0.05
SCALE_FLOOR = 0.01
LEARN_RATE = 0.05
OVER_ROWS = (((0,), (0,)), ((), ()))
MESH = pl.DeviceIdType.MESH
F32, BF16 = jnp.float32, jnp.bfloat16

SIDE = 4
FS = SIDE * SIDE
CHUNK = 256
SLOTS = 3
STEPS = (0, -1, 1, 2)


def kernel(
    tp,
    normed,
    query_cotangent,
    attended,
    output_cotangent,
    query_basis,
    output_basis,
    query_master,
    output_master,
    query_first,
    query_second,
    output_first,
    output_second,
    query_first_new,
    query_second_new,
    query_step,
    query_new,
    query_copy,
    output_first_new,
    output_second_new,
    output_step,
    output_new,
    output_copy,
    gathered,
    tokens,
    basis,
    cotangents,
    master,
    moment,
    lowered,
    partial,
    partial_out,
    partial_in,
    ratio_all,
    square_out,
    square_in,
    block_send,
    block_recv,
    part_send,
    part_recv,
    ratio_send,
    ratio_recv,
    square_send,
    square_recv,
    local_sem,
    token_sem,
    round_sem,
):
    fs_me = lax.axis_index("fs")
    tp_me = lax.axis_index("tp")
    y, x = fs_me // SIDE, fs_me % SIDE
    z, core = tp_me // 2, tp_me % 2
    heights = tp // 2

    def at(dy, dx):
        return ((y + dy + SIDE) % SIDE) * SIDE + (x + dx + SIDE) % SIDE

    def up(dz):
        return ((z + dz + heights) % heights) * 2 + core

    near = [{"fs": at(0, 1)}, {"fs": at(0, -1)}, {"fs": at(1, 0)}, {"fs": at(-1, 0)}]
    near += [{"tp": up(1)}, {"tp": up(-1)}, {"tp": z * 2 + (1 - core)}]

    def greet(sem):
        for device in near:
            pl.semaphore_signal(sem, inc=1, device_id=device, device_id_type=MESH)

    barrier = pltpu.get_barrier_semaphore()
    greet(barrier)

    loads = []
    for k, (src, dst) in enumerate(
        (
            (query_master, master.at[0]),
            (output_master, master.at[1]),
            (query_basis, basis.at[0]),
            (output_basis, basis.at[1]),
            (query_cotangent, cotangents.at[0]),
            (attended, cotangents.at[1]),
            (query_first, moment.at[0]),
            (query_second, moment.at[1]),
            (output_first, moment.at[2]),
            (output_second, moment.at[3]),
        )
    ):
        loads.append(pltpu.make_async_copy(src, dst, local_sem.at[k]))
    for load in loads[:3]:
        load.start()

    chunks = normed.shape[0] // CHUNK
    sources = (normed, output_cotangent)

    def token_load(which, chunk, slot):
        rows = sources[which].at[pl.ds(pl.multiple_of(chunk * CHUNK, CHUNK), CHUNK)]
        return pltpu.make_async_copy(rows, tokens.at[slot], token_sem.at[slot])

    for k in range(SLOTS):
        token_load(0, k, k).start()
    for load in loads[3:]:
        load.start()

    for w in range(2):
        loads[w].wait()
        gathered[w, fs_me] = master[w].astype(BF16)

    half = gathered.shape[2] // 2
    upper, lower, full = pl.ds(0, half), pl.ds(half, half), pl.ds(0, 2 * half)

    def place(w, da, db):
        return at(db, da) if w == 0 else at(da, db)

    def send(w, number, along_a, sign, block, rows):
        device = place(w, sign, 0) if along_a else place(w, 0, sign)
        piece = gathered.at[w, place(w, *block), rows]
        op = pltpu.make_async_remote_copy(
            src_ref=piece,
            dst_ref=piece,
            send_sem=block_send.at[w, number],
            recv_sem=block_recv.at[w, number],
            device_id={"fs": device},
            device_id_type=MESH,
        )
        op.start()
        return op

    sent = []

    def arrived(w, number, block, rows):
        piece = gathered.at[w, place(w, *block), rows]
        pltpu.make_async_remote_copy(
            src_ref=piece,
            dst_ref=piece,
            send_sem=block_send.at[w, number],
            recv_sem=block_recv.at[w, number],
            device_id={"fs": at(0, 1)},
            device_id_type=MESH,
        ).wait_recv()

    def first_own(w):
        sent.append(send(w, 0, True, 1, (0, 0), full))
        sent.append(send(w, 1, True, -1, (0, 0), full))

    def first_relay(w):
        arrived(w, 0, (-1, 0), full)
        sent.append(send(w, 2, True, 1, (-1, 0), upper))
        arrived(w, 1, (1, 0), full)
        sent.append(send(w, 3, True, -1, (1, 0), lower))

    def second_own(w, k):
        if k == 3:
            arrived(w, 2, (2, 0), upper)
            arrived(w, 3, (2, 0), lower)
        sent.append(send(w, 4 + 2 * k, False, 1, (STEPS[k], 0), full))
        sent.append(send(w, 5 + 2 * k, False, -1, (STEPS[k], 0), full))

    def second_relay(w, k):
        arrived(w, 4 + 2 * k, (STEPS[k], -1), full)
        sent.append(send(w, 12 + 2 * k, False, 1, (STEPS[k], -1), upper))
        arrived(w, 5 + 2 * k, (STEPS[k], 1), full)
        sent.append(send(w, 13 + 2 * k, False, -1, (STEPS[k], 1), lower))

    def second_last(w, k):
        arrived(w, 12 + 2 * k, (STEPS[k], 2), upper)
        arrived(w, 13 + 2 * k, (STEPS[k], 2), lower)

    pl.semaphore_wait(barrier, len(near))
    for w in range(2):
        first_own(w)
    for w in range(2):
        second_own(w, 0)

    def project(which, chunk, position):
        slot = lax.rem(position, SLOTS)
        token_load(which, chunk, slot).wait()
        low = jnp.dot(tokens[slot], basis[which], preferred_element_type=F32)
        high = low.astype(BF16)
        rest = (low - high.astype(F32)).astype(BF16)
        rows = pl.ds(pl.multiple_of(chunk * CHUNK, CHUNK), CHUNK)
        rank = low.shape[1]
        lowered[which, rows, pl.ds(0, rank)] = high
        lowered[which, rows, pl.ds(rank, rank)] = rest
        later = position + SLOTS

        @pl.when(later < chunks)
        def _():
            token_load(0, later, slot).start()

        @pl.when(jnp.logical_and(later >= chunks, later < 2 * chunks))
        def _():
            token_load(1, later - chunks, slot).start()

    def pair(which, number):
        greet(round_sem.at[2 * which + number])
        for k in range(2):
            chunk = 2 * number + k
            project(which, chunk, which * chunks + chunk)
        pl.semaphore_wait(round_sem.at[2 * which + number], len(near))

    def finish(which):
        both = lax.dot_general(
            lowered[which], cotangents[which], OVER_ROWS, preferred_element_type=F32
        )
        rank = both.shape[0] // 2
        total = both[:rank] + both[rank:]
        partial[which] = total.reshape(FS, rank // FS, total.shape[1])

    loads[2].wait()

    @pl.loop(0, 2)
    def _(number):
        pair(0, number)

    for load in loads[3:]:
        load.wait()
    finish(0)

    @pl.loop(0, 1)
    def _(number):
        pair(1, number)

    for w in range(2):
        first_relay(w)

    @pl.loop(1, 2)
    def _(number):
        pair(1, number)

    finish(1)
    partial_out[...] = jnp.concatenate([partial[0], partial[1]], axis=1).astype(BF16)

    part_ops = []
    for j in range(1, FS):
        target = lax.rem(fs_me + j, FS)
        op = pltpu.make_async_remote_copy(
            src_ref=partial_out.at[target],
            dst_ref=partial_in.at[j],
            send_sem=part_send.at[j],
            recv_sem=part_recv.at[j],
            device_id={"fs": target},
            device_id_type=MESH,
        )
        op.start()
        part_ops.append(op)

    for w in range(2):
        second_own(w, 1)

    grams = []
    for w in range(2):
        gram = lax.dot_general(basis[w], basis[w], OVER_ROWS, preferred_element_type=F32)
        grams.append(gram)

    for op in part_ops:
        op.wait_recv()
    incoming = jnp.sum(partial_in[pl.ds(1, FS - 1)].astype(F32), axis=0)
    outputs = (
        (query_first_new, query_second_new, query_step, query_new, query_copy),
        (output_first_new, output_second_new, output_step, output_new, output_copy),
    )
    ratios = []
    for w in range(2):
        own = partial[w, fs_me]
        rank_rows = own.shape[0]
        low = own + incoming[w * rank_rows : (w + 1) * rank_rows]
        first_new = FIRST_DECAY * moment[2 * w] + (1.0 - FIRST_DECAY) * low
        second_new = SECOND_DECAY * moment[2 * w + 1] + (1.0 - SECOND_DECAY) * low * low
        outputs[w][0][...] = first_new
        outputs[w][1][...] = second_new
        ratios.append(first_new / jnp.sqrt(second_new + SECOND_FLOOR))
    ratio_all[fs_me] = jnp.concatenate(ratios, axis=0).astype(BF16)

    ratio_ops = []
    for j in range(1, FS):
        op = pltpu.make_async_remote_copy(
            src_ref=ratio_all.at[fs_me],
            dst_ref=ratio_all.at[fs_me],
            send_sem=ratio_send.at[j],
            recv_sem=ratio_recv.at[j],
            device_id={"fs": lax.rem(fs_me + j, FS)},
            device_id_type=MESH,
        )
        op.start()
        ratio_ops.append(op)

    for k in (2, 3):
        for w in range(2):
            second_own(w, k)
    for w in range(2):
        second_relay(w, 0)

    for j in range(1, FS):
        source = lax.rem(fs_me + FS - j, FS)
        pltpu.make_async_remote_copy(
            src_ref=ratio_all.at[source],
            dst_ref=ratio_all.at[source],
            send_sem=ratio_send.at[j],
            recv_sem=ratio_recv.at[j],
            device_id={"fs": lax.rem(fs_me + j, FS)},
            device_id_type=MESH,
        ).wait_recv()
    every = ratio_all[...].astype(F32)
    rank_rows = every.shape[1] // 2
    full_ratio = []
    squares = []
    for w in range(2):
        ratio = every[:, w * rank_rows : (w + 1) * rank_rows, :].reshape(-1, every.shape[2])
        ratio_low = ratio.astype(BF16)
        full_ratio.append(ratio_low)
        high = grams[w].astype(BF16)
        rest = (grams[w] - high.astype(F32)).astype(BF16)
        spread = jnp.dot(high, ratio_low, preferred_element_type=F32)
        spread += jnp.dot(rest, ratio_low, preferred_element_type=F32)
        squares.append(jnp.sum(ratio * spread))
    row = lax.broadcasted_iota(jnp.int32, square_out.shape, 0)
    shares = jnp.where(row < 4, squares[0], squares[1])
    square_out[...] = shares
    square_in[0] = shares

    square_ops = []
    for j in range(1, tp):
        op = pltpu.make_async_remote_copy(
            src_ref=square_out,
            dst_ref=square_in.at[j],
            send_sem=square_send.at[j],
            recv_sem=square_recv.at[j],
            device_id={"tp": lax.rem(tp_me + j, tp)},
            device_id_type=MESH,
        )
        op.start()
        square_ops.append(op)

    for k in (1, 2):
        for w in range(2):
            second_relay(w, k)

    for op in square_ops:
        op.wait_recv()
    entries = basis.shape[1] * full_ratio[0].shape[1] * tp
    factors = lax.rsqrt(jnp.sum(square_in[...], axis=0) / entries + SCALE_FLOOR)
    scale = [factors[0:1, 0:1], factors[4:5, 0:1]]

    block_rows = gathered.shape[2]

    def updated(w, owner):
        rows = pl.ds(pl.multiple_of(owner * block_rows, block_rows), block_rows)
        update = jnp.dot(basis[w, rows], full_ratio[w], preferred_element_type=F32)
        return update * scale[w]

    def settle(w, block):
        owner = place(w, *block)
        step = updated(w, owner)
        new = gathered[w, owner].astype(F32) - LEARN_RATE * step
        outputs[w][4][owner] = new.astype(BF16)

    for w in range(2):
        step = updated(w, fs_me)
        new = master[w] - LEARN_RATE * step
        outputs[w][2][...] = step
        outputs[w][3][...] = new
        outputs[w][4][fs_me] = new.astype(BF16)
        for da in (-1, 1, 2):
            settle(w, (da, 0))
        for k in range(3):
            for db in (-1, 1):
                settle(w, (STEPS[k], db))

    for w in range(2):
        second_relay(w, 3)
    for w in range(2):
        for db in (-1, 1):
            settle(w, (STEPS[3], db))
    for k in range(4):
        for w in range(2):
            second_last(w, k)
            settle(w, (STEPS[k], 2))

    for op in sent + part_ops + ratio_ops + square_ops:
        op.wait_send()


def spread_kernel(count, *refs):
    sources, targets, sem = refs[:count], refs[count : 2 * count], refs[2 * count]
    copies = []
    for k in range(count):
        copies.append(pltpu.make_async_copy(sources[k], targets[k], sem.at[k]))
    for copy in copies:
        copy.start()
    for copy in copies:
        copy.wait()


def body(
    normed,
    query_cotangent,
    attended,
    output_cotangent,
    query_basis,
    output_basis,
    query_master,
    output_master,
    query_first,
    query_second,
    output_first,
    output_second,
):
    operands = (
        normed,
        query_cotangent,
        attended,
        output_cotangent,
        query_basis,
        output_basis,
        query_master,
        output_master,
        query_first,
        query_second,
        output_first,
        output_second,
    )
    tp = lax.axis_size("tp")
    token_rows, width = normed.shape
    rank = query_basis.shape[1]
    rows, columns = query_master.shape
    rank_rows = query_first.shape[0]
    per_weight = (
        ((rank_rows, columns), F32),
        ((rank_rows, columns), F32),
        ((rows, columns), F32),
        ((rows, columns), F32),
        ((FS, rows, columns), BF16),
    )
    results = pl.pallas_call(
        lambda *refs: kernel(tp, *refs),
        out_shape=[pltpu.VMEM(s, d) for s, d in per_weight * 2],
        in_specs=[pl.BlockSpec(memory_space=pltpu.HBM)] * 12,
        out_specs=[pl.BlockSpec(memory_space=pltpu.VMEM)] * 10,
        scratch_shapes=[
            pltpu.VMEM((2, FS, rows, columns), BF16),
            pltpu.VMEM((SLOTS, CHUNK, width), BF16),
            pltpu.VMEM((2, width, rank), BF16),
            pltpu.VMEM((2, token_rows, columns), BF16),
            pltpu.VMEM((2, rows, columns), F32),
            pltpu.VMEM((4, rank_rows, columns), F32),
            pltpu.VMEM((2, token_rows, 2 * rank), BF16),
            pltpu.VMEM((2, FS, rank_rows, columns), F32),
            pltpu.VMEM((FS, 2 * rank_rows, columns), BF16),
            pltpu.VMEM((FS, 2 * rank_rows, columns), BF16),
            pltpu.VMEM((FS, 2 * rank_rows, columns), BF16),
            pltpu.VMEM((8, 128), F32),
            pltpu.VMEM((tp, 8, 128), F32),
            pltpu.SemaphoreType.DMA((2, 20)),
            pltpu.SemaphoreType.DMA((2, 20)),
            pltpu.SemaphoreType.DMA((FS,)),
            pltpu.SemaphoreType.DMA((FS,)),
            pltpu.SemaphoreType.DMA((FS,)),
            pltpu.SemaphoreType.DMA((FS,)),
            pltpu.SemaphoreType.DMA((tp,)),
            pltpu.SemaphoreType.DMA((tp,)),
            pltpu.SemaphoreType.DMA((10,)),
            pltpu.SemaphoreType.DMA((SLOTS,)),
            pltpu.SemaphoreType.REGULAR((4,)),
        ],
        compiler_params=pltpu.CompilerParams(
            collective_id=0, has_side_effects=True, vmem_limit_bytes=40 * 1024 * 1024
        ),
        name="exchange",
    )(*(pltpu.with_memory_space_constraint(operand, pltpu.HBM) for operand in operands))
    count = len(results)
    results = pl.pallas_call(
        lambda *refs: spread_kernel(count, *refs),
        out_shape=[jax.ShapeDtypeStruct(r.shape, r.dtype) for r in results],
        in_specs=[pl.BlockSpec(memory_space=pltpu.VMEM)] * count,
        out_specs=[pl.BlockSpec(memory_space=pl.ANY)] * count,
        scratch_shapes=[pltpu.SemaphoreType.DMA((count,))],
        compiler_params=pltpu.CompilerParams(vmem_limit_bytes=8 * 1024 * 1024),
        name="store",
    )(*results)
    return tuple(r.reshape(-1, columns) for r in results)


def solution(mesh):
    in_specs = (
        P("fs", None),
        P("fs", "tp"),
        P("fs", "tp"),
        P("fs", None),
        P(),
        P(),
        P("fs", "tp"),
        P("fs", "tp"),
        P("fs", "tp"),
        P("fs", "tp"),
        P("fs", "tp"),
        P("fs", "tp"),
    )
    out_specs = (
        P("fs", "tp"),
        P("fs", "tp"),
        P("fs", "tp"),
        P("fs", "tp"),
        P(None, "tp"),
        P("fs", "tp"),
        P("fs", "tp"),
        P("fs", "tp"),
        P("fs", "tp"),
        P(None, "tp"),
    )
    return jax.shard_map(body, mesh=mesh, in_specs=in_specs, out_specs=out_specs, check_vma=False)
```

time: 159 us -> 44.1 us (0.28)
  waiting for transfers between devices: 63.5 us -> 0 us
  Pallas kernels: 0 us -> 43.4 us
  starting transfers between devices: 23.5 us -> 0 us
  local copies, waits for them, and re-layouts: 18.9 us -> 0 us
  matrix products: 17.5 us -> 0 us
  blocking collectives: 16.4 us -> 0 us
  between operations: 15.7 us -> 0.66 us
  other arithmetic: 2.78 us -> 0 us
    all_gather x1 -> x0, waiting for transfers between devices: 50.3 us -> none  [side_by_side(): lax.all_gather(both, axis, axis=dim, tiled=True)]
    pallas_call x0 -> x2, Pallas kernels: none -> 43.4 us  [the longest x1 40.9 us: body(): pl.pallas_call(lambda *refs: kernel(tp, *refs), out_shape=[pltpu.VMEM(s,...]
    all_to_all x2 -> x0, starting transfers between devices: 23.5 us -> none  [the longest x1 15.9 us: copy_for_each(): return lax.all_to_all(copies, axis, split_axis=0, concat_axis=0, tiled=True)]
    dot_general x14 -> x0, matrix products: 17.5 us -> none  [the longest x1 6.14 us: body(): lax.dot_general(normed, query_cotangent, CONTRACT, preferred_element_type...]
    all_gather x1 -> x0, blocking collectives: 16.4 us -> none  [side_by_side(): lax.all_gather(both, axis, axis=dim, tiled=True)]
    all_to_all x2 -> x0, waiting for transfers between devices: 13.2 us -> none  [the longest x1 6.63 us: copy_for_each(): return lax.all_to_all(copies, axis, split_axis=0, concat_axis=0, tiled=True)]
    unnamed x28 -> x0, local copies, waits for them, and re-layouts: 12.9 us -> none
    split x1 -> x0, local copies, waits for them, and re-layouts: 3.92 us -> none  [side_by_side(): jnp.split(lax.all_gather(both, axis, axis=dim, tiled=True), ends, axis=al...]
  transfers between devices with their start and end apart: 3 -> 0, of which waited for: 3 -> 0; matrix products, arithmetic and copies ran while one was open for 3% -> 0% of each run, Pallas kernels for 0% -> 0%
where the time goes in v1:
time: 44.1 us; the launch traced here: 44 us
  Pallas kernels  43.4 us (98%)
  between operations  0.66 us (1%)
    pallas_call x1, Pallas kernels, body(): pl.pallas_call(lambda *refs: kernel(tp, *refs), out_shape=[pltpu.VMEM(s,...  40.9 us
    pallas_call x1, Pallas kernels, body(): pl.pallas_call(lambda *refs: spread_kernel(count, *refs), out_shape=[jax....  2.47 us

profile of v1, /device:TPU:1, one launch (start us, length us, event | category | flops | bytes accessed | tf_op | source)
XLA Modules:
  0.0 44.0 jit_solution(8389991757310564764)
XLA Ops:
  0.6 40.9 %exchange.1 = (f32[8,256]{1,0:T(8,128)S(1)}, f32[8,256]{1,0:T(8,128)S(1)}, f32[256,256]{1,0:T(8,128)S(1)}, f32[256,256]{1,0:T(8,128)S(1)}, bf16[16,256,256]{2,1,...) custom-call(bf16[1024,4096]{1,0:T(8,128)(2,1)} %refs_0_.1, ...), custom_call_target="tpu_custom_call" | custom-call | tf_op jit(solution)/shard_map/exchange/pallas_call | solution.py:456
  41.6 2.5 %store.1 = (f32[8,256]{1,0:T(8,128)}, f32[8,256]{1,0:T(8,128)}, f32[256,256]{1,0:T(8,128)}, f32[256,256]{1,0:T(8,128)}, bf16[16,256,256]{2,1,0:T(8,128)(2,1)}, /...) custom-call(f32[8,256]{1,0:T(8,128)S(1)} %get-tuple-element.30.refs_, ...), custom_call_target="tpu_custom_call" | custom-call | tf_op jit(solution)/shard_map/store/pallas_call | solution.py:493

commit v2 on v1

--- a/solution.py
+++ b/solution.py
@@ -17,7 +17,7 @@
 SIDE = 4
 FS = SIDE * SIDE
 CHUNK = 256
-SLOTS = 3
+UPPER = 128
 STEPS = (0, -1, 1, 2)
 
 
@@ -56,6 +56,7 @@
     partial_out,
     partial_in,
     ratio_all,
+    update,
     square_out,
     square_in,
     block_send,
@@ -66,9 +67,11 @@
     ratio_recv,
     square_send,
     square_recv,
+    half_send,
+    half_recv,
     local_sem,
-    token_sem,
     round_sem,
+    entered,
 ):
     fs_me = lax.axis_index("fs")
     tp_me = lax.axis_index("tp")
@@ -83,52 +86,62 @@
         return ((z + dz + heights) % heights) * 2 + core
 
     near = [{"fs": at(0, 1)}, {"fs": at(0, -1)}, {"fs": at(1, 0)}, {"fs": at(-1, 0)}]
-    near += [{"tp": up(1)}, {"tp": up(-1)}, {"tp": z * 2 + (1 - core)}]
+    partner = {"tp": z * 2 + (1 - core)}
+
+    def tell(sem, device):
+        pl.semaphore_signal(sem, inc=1, device_id=device, device_id_type=MESH)
 
     def greet(sem):
         for device in near:
-            pl.semaphore_signal(sem, inc=1, device_id=device, device_id_type=MESH)
+            tell(sem, device)
 
     barrier = pltpu.get_barrier_semaphore()
     greet(barrier)
-
+    tell(barrier, partner)
+    for dz in range(1, heights):
+
+        @pl.when(z + dz < heights)
+        def _():
+            for c in range(2):
+                tell(barrier, {"tp": (z + dz) * 2 + c})
+
+    sources = (normed, output_cotangent)
+    share = normed.shape[0] // 2
+    chunks = share // CHUNK
+
+    def token_rows(chunk, of=core):
+        return pl.ds(pl.multiple_of(of * share + chunk * CHUNK, CHUNK), CHUNK)
+
+    pieces = [
+        (query_master, master.at[0]),
+        (output_master, master.at[1]),
+        (query_basis, basis.at[0]),
+    ]
+    for w in range(2):
+        for k in range(chunks):
+            pieces.append((sources[w].at[token_rows(k)], tokens.at[w, k]))
+        if w == 0:
+            pieces.append((query_cotangent, cotangents.at[0]))
+            pieces.append((output_basis, basis.at[1]))
+        else:
+            pieces.append((attended, cotangents.at[1]))
+    pieces += [
+        (query_first, moment.at[0]),
+        (query_second, moment.at[1]),
+        (output_first, moment.at[2]),
+        (output_second, moment.at[3]),
+    ]
     loads = []
-    for k, (src, dst) in enumerate(
-        (
-            (query_master, master.at[0]),
-            (output_master, master.at[1]),
-            (query_basis, basis.at[0]),
-            (output_basis, basis.at[1]),
-            (query_cotangent, cotangents.at[0]),
-            (attended, cotangents.at[1]),
-            (query_first, moment.at[0]),
-            (query_second, moment.at[1]),
-            (output_first, moment.at[2]),
-            (output_second, moment.at[3]),
-        )
-    ):
+    for k, (src, dst) in enumerate(pieces):
         loads.append(pltpu.make_async_copy(src, dst, local_sem.at[k]))
-    for load in loads[:3]:
-        load.start()
-
-    chunks = normed.shape[0] // CHUNK
-    sources = (normed, output_cotangent)
-
-    def token_load(which, chunk, slot):
-        rows = sources[which].at[pl.ds(pl.multiple_of(chunk * CHUNK, CHUNK), CHUNK)]
-        return pltpu.make_async_copy(rows, tokens.at[slot], token_sem.at[slot])
-
-    for k in range(SLOTS):
-        token_load(0, k, k).start()
-    for load in loads[3:]:
-        load.start()
+        loads[-1].start()
 
     for w in range(2):
         loads[w].wait()
         gathered[w, fs_me] = master[w].astype(BF16)
 
-    half = gathered.shape[2] // 2
-    upper, lower, full = pl.ds(0, half), pl.ds(half, half), pl.ds(0, 2 * half)
+    rows = gathered.shape[2]
+    upper, lower, full = pl.ds(0, UPPER), pl.ds(UPPER, rows - UPPER), pl.ds(0, rows)
 
     def place(w, da, db):
         return at(db, da) if w == 0 else at(da, db)
@@ -187,70 +200,75 @@
         arrived(w, 12 + 2 * k, (STEPS[k], 2), upper)
         arrived(w, 13 + 2 * k, (STEPS[k], 2), lower)
 
-    pl.semaphore_wait(barrier, len(near))
+    pl.semaphore_wait(barrier, len(near) + 1 + 2 * z)
     for w in range(2):
         first_own(w)
     for w in range(2):
         second_own(w, 0)
-
-    def project(which, chunk, position):
-        slot = lax.rem(position, SLOTS)
-        token_load(which, chunk, slot).wait()
-        low = jnp.dot(tokens[slot], basis[which], preferred_element_type=F32)
+    greet(round_sem.at[0])
+    for dz in range(1, heights):
+
+        @pl.when(z - dz >= 0)
+        def _():
+            for c in range(2):
+                tell(entered, {"tp": (z - dz) * 2 + c})
+
+    halves = []
+
+    def hand_over(w, k, of):
+        return pltpu.make_async_remote_copy(
+            src_ref=lowered.at[w, token_rows(k, of)],
+            dst_ref=lowered.at[w, token_rows(k, of)],
+            send_sem=half_send.at[w, k],
+            recv_sem=half_recv.at[w, k],
+            device_id=partner,
+            device_id_type=MESH,
+        )
+
+    def project(w, k):
+        low = jnp.dot(tokens[w, k], basis[w], preferred_element_type=F32)
         high = low.astype(BF16)
         rest = (low - high.astype(F32)).astype(BF16)
-        rows = pl.ds(pl.multiple_of(chunk * CHUNK, CHUNK), CHUNK)
         rank = low.shape[1]
-        lowered[which, rows, pl.ds(0, rank)] = high
-        lowered[which, rows, pl.ds(rank, rank)] = rest
-        later = position + SLOTS
-
-        @pl.when(later < chunks)
-        def _():
-            token_load(0, later, slot).start()
-
-        @pl.when(jnp.logical_and(later >= chunks, later < 2 * chunks))
-        def _():
-            token_load(1, later - chunks, slot).start()
-
-    def pair(which, number):
-        greet(round_sem.at[2 * which + number])
-        for k in range(2):
-            chunk = 2 * number + k
-            project(which, chunk, which * chunks + chunk)
-        pl.semaphore_wait(round_sem.at[2 * which + number], len(near))
-
-    def finish(which):
+        lowered[w, token_rows(k), pl.ds(0, rank)] = high
+        lowered[w, token_rows(k), pl.ds(rank, rank)] = rest
+        op = hand_over(w, k, core)
+        op.start()
+        halves.append(op)
+
+    def finish(w):
+        for k in range(chunks):
+            hand_over(w, k, 1 - core).wait_recv()
         both = lax.dot_general(
-            lowered[which], cotangents[which], OVER_ROWS, preferred_element_type=F32
+            lowered[w], cotangents[w], OVER_ROWS, preferred_element_type=F32
         )
         rank = both.shape[0] // 2
         total = both[:rank] + both[rank:]
-        partial[which] = total.reshape(FS, rank // FS, total.shape[1])
+        partial[w] = total.reshape(FS, rank // FS, total.shape[1])
+
+    def next_round(k):
+        pl.semaphore_wait(round_sem.at[k], len(near))
+        if k < 2:
+            greet(round_sem.at[k + 1])
 
     loads[2].wait()
-
-    @pl.loop(0, 2)
-    def _(number):
-        pair(0, number)
-
-    for load in loads[3:]:
-        load.wait()
+    loads[3].wait()
+    project(0, 0)
+    loads[4].wait()
+    project(0, 1)
+    next_round(0)
+    loads[5].wait()
+    loads[6].wait()
+    loads[7].wait()
+    project(1, 0)
     finish(0)
-
-    @pl.loop(0, 1)
-    def _(number):
-        pair(1, number)
-
-    for w in range(2):
-        first_relay(w)
-
-    @pl.loop(1, 2)
-    def _(number):
-        pair(1, number)
-
+    next_round(1)
+    loads[8].wait()
+    project(1, 1)
+    loads[9].wait()
     finish(1)
     partial_out[...] = jnp.concatenate([partial[0], partial[1]], axis=1).astype(BF16)
+    next_round(2)
 
     part_ops = []
     for j in range(1, FS):
@@ -267,6 +285,8 @@
         part_ops.append(op)
 
     for w in range(2):
+        first_relay(w)
+    for w in range(2):
         second_own(w, 1)
 
     grams = []
@@ -274,6 +294,8 @@
         gram = lax.dot_general(basis[w], basis[w], OVER_ROWS, preferred_element_type=F32)
         grams.append(gram)
 
+    for load in loads[10:]:
+        load.wait()
     for op in part_ops:
         op.wait_recv()
     incoming = jnp.sum(partial_in[pl.ds(1, FS - 1)].astype(F32), axis=0)
@@ -340,6 +362,10 @@
     square_out[...] = shares
     square_in[0] = shares
 
+    @pl.when(z < heights - 1)
+    def _():
+        pl.semaphore_wait(entered, 2 * (heights - 1 - z))
+
     square_ops = []
     for j in range(1, tp):
         op = pltpu.make_async_remote_copy(
@@ -353,7 +379,14 @@
         op.start()
         square_ops.append(op)
 
-    for k in (1, 2):
+    @pl.loop(0, FS // 2)
+    def _(k):
+        for w in range(2):
+            pair = pl.ds(pl.multiple_of(2 * rows * k, 2 * rows), 2 * rows)
+            product = jnp.dot(basis[w, pair], full_ratio[w], preferred_element_type=F32)
+            update[w, pl.ds(2 * k, 2)] = product.reshape(2, rows, product.shape[1])
+
+    for k in (1, 2, 3):
         for w in range(2):
             second_relay(w, k)
 
@@ -363,52 +396,45 @@
     factors = lax.rsqrt(jnp.sum(square_in[...], axis=0) / entries + SCALE_FLOOR)
     scale = [factors[0:1, 0:1], factors[4:5, 0:1]]
 
-    block_rows = gathered.shape[2]
-
-    def updated(w, owner):
-        rows = pl.ds(pl.multiple_of(owner * block_rows, block_rows), block_rows)
-        update = jnp.dot(basis[w, rows], full_ratio[w], preferred_element_type=F32)
-        return update * scale[w]
-
-    def settle(w, block):
-        owner = place(w, *block)
-        step = updated(w, owner)
-        new = gathered[w, owner].astype(F32) - LEARN_RATE * step
+    def settle(w, da, db):
+        owner = place(w, da, db)
+        new = gathered[w, owner].astype(F32) - (LEARN_RATE * scale[w]) * update[w, owner]
         outputs[w][4][owner] = new.astype(BF16)
 
-    for w in range(2):
-        step = updated(w, fs_me)
+    @pl.loop(1, 3 * SIDE)
+    def _(k):
+        db = lax.rem(k // SIDE + 1, 3) - 1
+        for w in range(2):
+            settle(w, lax.rem(k, SIDE), db)
+
+    for w in range(2):
+        step = update[w, fs_me] * scale[w]
         new = master[w] - LEARN_RATE * step
         outputs[w][2][...] = step
         outputs[w][3][...] = new
         outputs[w][4][fs_me] = new.astype(BF16)
-        for da in (-1, 1, 2):
-            settle(w, (da, 0))
-        for k in range(3):
-            for db in (-1, 1):
-                settle(w, (STEPS[k], db))
-
-    for w in range(2):
-        second_relay(w, 3)
-    for w in range(2):
-        for db in (-1, 1):
-            settle(w, (STEPS[3], db))
+
     for k in range(4):
         for w in range(2):
             second_last(w, k)
-            settle(w, (STEPS[k], 2))
-
-    for op in sent + part_ops + ratio_ops + square_ops:
+            settle(w, STEPS[k], 2)
+
+    for op in sent + halves + part_ops + ratio_ops + square_ops:
         op.wait_send()
 
 
-def spread_kernel(count, *refs):
+def store_kernel(count, *refs):
     sources, targets, sem = refs[:count], refs[count : 2 * count], refs[2 * count]
     copies = []
     for k in range(count):
-        copies.append(pltpu.make_async_copy(sources[k], targets[k], sem.at[k]))
-    for copy in copies:
-        copy.start()
+        pieces = 4 if len(sources[k].shape) == 3 else 1
+        size = sources[k].shape[0] // pieces
+        for p in range(pieces):
+            part = pl.ds(p * size, size)
+            copies.append(
+                pltpu.make_async_copy(sources[k].at[part], targets[k].at[part], sem.at[len(copies)])
+            )
+            copies[-1].start()
     for copy in copies:
         copy.wait()
 
@@ -460,7 +486,7 @@
         out_specs=[pl.BlockSpec(memory_space=pltpu.VMEM)] * 10,
         scratch_shapes=[
             pltpu.VMEM((2, FS, rows, columns), BF16),
-            pltpu.VMEM((SLOTS, CHUNK, width), BF16),
+            pltpu.VMEM((2, token_rows // 2 // CHUNK, CHUNK, width), BF16),
             pltpu.VMEM((2, width, rank), BF16),
             pltpu.VMEM((2, token_rows, columns), BF16),
             pltpu.VMEM((2, rows, columns), F32),
@@ -470,6 +496,7 @@
             pltpu.VMEM((FS, 2 * rank_rows, columns), BF16),
             pltpu.VMEM((FS, 2 * rank_rows, columns), BF16),
             pltpu.VMEM((FS, 2 * rank_rows, columns), BF16),
+            pltpu.VMEM((2, FS, rows, columns), F32),
             pltpu.VMEM((8, 128), F32),
             pltpu.VMEM((tp, 8, 128), F32),
             pltpu.SemaphoreType.DMA((2, 20)),
@@ -480,9 +507,11 @@
             pltpu.SemaphoreType.DMA((FS,)),
             pltpu.SemaphoreType.DMA((tp,)),
             pltpu.SemaphoreType.DMA((tp,)),
-            pltpu.SemaphoreType.DMA((10,)),
-            pltpu.SemaphoreType.DMA((SLOTS,)),
-            pltpu.SemaphoreType.REGULAR((4,)),
+            pltpu.SemaphoreType.DMA((2, token_rows // 2 // CHUNK)),
+            pltpu.SemaphoreType.DMA((2, token_rows // 2 // CHUNK)),
+            pltpu.SemaphoreType.DMA((14,)),
+            pltpu.SemaphoreType.REGULAR((3,)),
+            pltpu.SemaphoreType.REGULAR,
         ],
         compiler_params=pltpu.CompilerParams(
             collective_id=0, has_side_effects=True, vmem_limit_bytes=40 * 1024 * 1024
@@ -491,11 +520,11 @@
     )(*(pltpu.with_memory_space_constraint(operand, pltpu.HBM) for operand in operands))
     count = len(results)
     results = pl.pallas_call(
-        lambda *refs: spread_kernel(count, *refs),
+        lambda *refs: store_kernel(count, *refs),
         out_shape=[jax.ShapeDtypeStruct(r.shape, r.dtype) for r in results],
         in_specs=[pl.BlockSpec(memory_space=pltpu.VMEM)] * count,
         out_specs=[pl.BlockSpec(memory_space=pl.ANY)] * count,
-        scratch_shapes=[pltpu.SemaphoreType.DMA((count,))],
+        scratch_shapes=[pltpu.SemaphoreType.DMA((2 * count,))],
         compiler_params=pltpu.CompilerParams(vmem_limit_bytes=8 * 1024 * 1024),
         name="store",
     )(*results)

time: 44.1 us -> 38.8 us (0.88)
  Pallas kernels: 43.4 us -> 38.1 us
    pallas_call x1, Pallas kernels: 40.9 us -> 35.6 us  [body(): pl.pallas_call(lambda *refs: kernel(tp, *refs), out_shape=[pltpu.VMEM(s,...]
where the time goes in v2:
time: 38.8 us
  Pallas kernels  38.1 us (98%)
  between operations  0.66 us (2%)
    pallas_call x1, Pallas kernels, body(): pl.pallas_call(lambda *refs: kernel(tp, *refs), out_shape=[pltpu.VMEM(s,...  35.6 us
    pallas_call x1, Pallas kernels, body(): pl.pallas_call(lambda *refs: store_kernel(count, *refs), out_shape=[jax.S...  2.53 us

profile of v2, /device:TPU:1, one launch (start us, length us, event | category | flops | bytes accessed | tf_op | source)
XLA Modules:
  0.0 38.8 jit_solution(7482612498385553222)
XLA Ops:
  0.6 35.6 %exchange.1 = (f32[8,256]{1,0:T(8,128)S(1)}, f32[8,256]{1,0:T(8,128)S(1)}, f32[256,256]{1,0:T(8,128)S(1)}, f32[256,256]{1,0:T(8,128)S(1)}, bf16[16,256,256]{2,1,...) custom-call(bf16[1024,4096]{1,0:T(8,128)(2,1)} %refs_0_.1, ...), custom_call_target="tpu_custom_call" | custom-call | tf_op jit(solution)/shard_map/exchange/pallas_call | solution.py:482
  36.2 2.5 %store.1 = (f32[8,256]{1,0:T(8,128)}, f32[8,256]{1,0:T(8,128)}, f32[256,256]{1,0:T(8,128)}, f32[256,256]{1,0:T(8,128)}, bf16[16,256,256]{2,1,0:T(8,128)(2,1)}, /...) custom-call(f32[8,256]{1,0:T(8,128)S(1)} %get-tuple-element.30.refs_, ...), custom_call_target="tpu_custom_call" | custom-call | tf_op jit(solution)/shard_map/store/pallas_call | solution.py:522

commit v3 on v2

v3 whole, which is shorter than its diff:
```python
import jax
import jax.numpy as jnp
from jax import lax
from jax.experimental import pallas as pl
from jax.experimental.pallas import tpu as pltpu
from jax.sharding import PartitionSpec as P

FIRST_DECAY = 0.7
SECOND_DECAY = 0.8
SECOND_FLOOR = 0.05
SCALE_FLOOR = 0.01
LEARN_RATE = 0.05
OVER_ROWS = (((0,), (0,)), ((), ()))
MESH = pl.DeviceIdType.MESH
F32, BF16 = jnp.float32, jnp.bfloat16

SIDE = 4
FS = SIDE * SIDE
CHUNK = 128
UPPER = 128
STEPS = (0, -1, 1, 2)


def kernel(
    tp,
    normed,
    query_cotangent,
    attended,
    output_cotangent,
    query_basis,
    output_basis,
    query_master,
    output_master,
    query_first,
    query_second,
    output_first,
    output_second,
    gathered,
    update,
    own_update,
    master,
    scales,
    query_first_new,
    query_second_new,
    output_first_new,
    output_second_new,
    tokens,
    basis,
    cotangents,
    moment,
    lowered,
    partial,
    partial_out,
    partial_in,
    ratio_all,
    square_out,
    square_in,
    block_send,
    block_recv,
    part_send,
    part_recv,
    ratio_send,
    ratio_recv,
    square_send,
    square_recv,
    half_send,
    half_recv,
    local_sem,
    round_sem,
    entered,
):
    fs_me = lax.axis_index("fs")
    tp_me = lax.axis_index("tp")
    y, x = fs_me // SIDE, fs_me % SIDE
    z, core = tp_me // 2, tp_me % 2
    heights = tp // 2

    def at(dy, dx):
        return ((y + dy + SIDE) % SIDE) * SIDE + (x + dx + SIDE) % SIDE

    def up(dz):
        return ((z + dz + heights) % heights) * 2 + core

    near = [{"fs": at(0, 1)}, {"fs": at(0, -1)}, {"fs": at(1, 0)}, {"fs": at(-1, 0)}]
    partner = {"tp": z * 2 + (1 - core)}

    def tell(sem, device):
        pl.semaphore_signal(sem, inc=1, device_id=device, device_id_type=MESH)

    def greet(sem):
        for device in near:
            tell(sem, device)

    barrier = pltpu.get_barrier_semaphore()
    greet(barrier)
    tell(barrier, partner)
    for dz in range(1, heights):

        @pl.when(z + dz < heights)
        def _():
            for c in range(2):
                tell(barrier, {"tp": (z + dz) * 2 + c})

    sources = (normed, output_cotangent)
    share = normed.shape[0] // 2
    chunks = share // CHUNK

    def token_rows(chunk, of=core):
        return pl.ds(pl.multiple_of(of * share + chunk * CHUNK, CHUNK), CHUNK)

    pieces = [
        (query_master, master.at[0]),
        (output_master, master.at[1]),
        (query_basis, basis.at[0]),
    ]
    for w in range(2):
        for k in range(chunks):
            pieces.append((sources[w].at[token_rows(k)], tokens.at[w, k]))
        if w == 0:
            pieces.append((query_cotangent, cotangents.at[0]))
            pieces.append((output_basis, basis.at[1]))
        else:
            pieces.append((attended, cotangents.at[1]))
    pieces += [
        (query_first, moment.at[0]),
        (query_second, moment.at[1]),
        (output_first, moment.at[2]),
        (output_second, moment.at[3]),
    ]
    loads = []
    for k, (src, dst) in enumerate(pieces):
        loads.append(pltpu.make_async_copy(src, dst, local_sem.at[k]))
        loads[-1].start()

    for w in range(2):
        loads[w].wait()
        gathered[w, fs_me] = master[w].astype(BF16)

    rows = gathered.shape[2]
    upper, lower, full = pl.ds(0, UPPER), pl.ds(UPPER, rows - UPPER), pl.ds(0, rows)

    def place(w, da, db):
        return at(db, da) if w == 0 else at(da, db)

    def send(w, number, along_a, sign, block, rows):
        device = place(w, sign, 0) if along_a else place(w, 0, sign)
        piece = gathered.at[w, place(w, *block), rows]
        op = pltpu.make_async_remote_copy(
            src_ref=piece,
            dst_ref=piece,
            send_sem=block_send.at[w],
            recv_sem=block_recv.at[w, number],
            device_id={"fs": device},
            device_id_type=MESH,
        )
        op.start()

    def arrived(w, number, block, rows):
        piece = gathered.at[w, place(w, *block), rows]
        pltpu.make_async_remote_copy(
            src_ref=piece,
            dst_ref=piece,
            send_sem=block_send.at[w],
            recv_sem=block_recv.at[w, number],
            device_id={"fs": at(0, 1)},
            device_id_type=MESH,
        ).wait_recv()

    def first_own(w):
        send(w, 0, True, 1, (0, 0), full)
        send(w, 1, True, -1, (0, 0), full)

    def first_relay(w):
        arrived(w, 0, (-1, 0), full)
        send(w, 2, True, 1, (-1, 0), upper)
        arrived(w, 1, (1, 0), full)
        send(w, 3, True, -1, (1, 0), lower)

    def second_own(w, k):
        if k == 3:
            arrived(w, 2, (2, 0), upper)
            arrived(w, 3, (2, 0), lower)
        send(w, 4 + 2 * k, False, 1, (STEPS[k], 0), full)
        send(w, 5 + 2 * k, False, -1, (STEPS[k], 0), full)

    def second_relay(w, k):
        arrived(w, 4 + 2 * k, (STEPS[k], -1), full)
        send(w, 12 + 2 * k, False, 1, (STEPS[k], -1), upper)
        arrived(w, 5 + 2 * k, (STEPS[k], 1), full)
        send(w, 13 + 2 * k, False, -1, (STEPS[k], 1), lower)

    def second_last(w, k):
        arrived(w, 12 + 2 * k, (STEPS[k], 2), upper)
        arrived(w, 13 + 2 * k, (STEPS[k], 2), lower)

    pl.semaphore_wait(barrier, len(near) + 1 + 2 * z)
    for w in range(2):
        first_own(w)
    for w in range(2):
        second_own(w, 0)
    greet(round_sem.at[0])
    for dz in range(1, heights):

        @pl.when(z - dz >= 0)
        def _():
            for c in range(2):
                tell(entered, {"tp": (z - dz) * 2 + c})

    def hand_over(w, k, of):
        return pltpu.make_async_remote_copy(
            src_ref=lowered.at[w, token_rows(k, of)],
            dst_ref=lowered.at[w, token_rows(k, of)],
            send_sem=half_send,
            recv_sem=half_recv.at[w, k],
            device_id=partner,
            device_id_type=MESH,
        )

    def project(w, k):
        low = jnp.dot(tokens[w, k], basis[w], preferred_element_type=F32)
        high = low.astype(BF16)
        rest = (low - high.astype(F32)).astype(BF16)
        rank = low.shape[1]
        lowered[w, token_rows(k), pl.ds(0, rank)] = high
        lowered[w, token_rows(k), pl.ds(rank, rank)] = rest
        op = hand_over(w, k, core)
        op.start()

    def contract(w, of):
        half = pl.ds(pl.multiple_of(of * share, share), share)
        return lax.dot_general(
            lowered[w, half], cotangents[w, half], OVER_ROWS, preferred_element_type=F32
        )

    def finish(w):
        both = contract(w, core)
        for k in range(chunks):
            hand_over(w, k, 1 - core).wait_recv()
        both += contract(w, 1 - core)
        rank = both.shape[0] // 2
        total = both[:rank] + both[rank:]
        partial[w] = total.reshape(FS, rank // FS, total.shape[1])

    def next_round(k):
        pl.semaphore_wait(round_sem.at[k], len(near))
        if k < 2:
            greet(round_sem.at[k + 1])

    loads[2].wait()
    first = 3
    for w in range(2):
        if w == 1:
            loads[first].wait()
            loads[first + 1].wait()
            first += 2
        for k in range(chunks):
            loads[first + k].wait()
            project(w, k)
            if w == 1 and k == 0:
                next_round(0)
                finish(0)
            if w == 1 and k == 2:
                next_round(1)
        first += chunks
    loads[first].wait()
    finish(1)
    first += 1
    partial_out[...] = jnp.concatenate([partial[0], partial[1]], axis=1).astype(BF16)
    next_round(2)

    for j in range(1, FS):
        target = lax.rem(fs_me + j, FS)
        op = pltpu.make_async_remote_copy(
            src_ref=partial_out.at[target],
            dst_ref=partial_in.at[j],
            send_sem=part_send,
            recv_sem=part_recv,
            device_id={"fs": target},
            device_id_type=MESH,
        )
        op.start()

    for w in range(2):
        first_relay(w)
    for w in range(2):
        second_own(w, 1)

    grams = []
    for w in range(2):
        gram = lax.dot_general(basis[w], basis[w], OVER_ROWS, preferred_element_type=F32)
        grams.append(gram)

    for load in loads[first:]:
        load.wait()
    def together(refs, sems):
        return pltpu.make_async_remote_copy(
            src_ref=refs,
            dst_ref=refs,
            send_sem=sems[0],
            recv_sem=sems[1],
            device_id=partner,
            device_id_type=MESH,
        )

    others = pl.ds(1, FS - 1)
    parts = together(partial_in.at[others], (part_send, part_recv))
    parts.wait_recv()
    incoming = jnp.sum(partial_in[pl.ds(1, FS - 1)].astype(F32), axis=0)
    moments = (
        (query_first_new, query_second_new),
        (output_first_new, output_second_new),
    )
    ratios = []
    for w in range(2):
        own = partial[w, fs_me]
        rank_rows = own.shape[0]
        low = own + incoming[w * rank_rows : (w + 1) * rank_rows]
        first_new = FIRST_DECAY * moment[2 * w] + (1.0 - FIRST_DECAY) * low
        second_new = SECOND_DECAY * moment[2 * w + 1] + (1.0 - SECOND_DECAY) * low * low
        moments[w][0][...] = first_new
        moments[w][1][...] = second_new
        ratios.append(first_new / jnp.sqrt(second_new + SECOND_FLOOR))
    ratio_all[fs_me] = jnp.concatenate(ratios, axis=0).astype(BF16)

    for j in range(1, FS):
        op = pltpu.make_async_remote_copy(
            src_ref=ratio_all.at[fs_me],
            dst_ref=ratio_all.at[fs_me],
            send_sem=ratio_send,
            recv_sem=ratio_recv,
            device_id={"fs": lax.rem(fs_me + j, FS)},
            device_id_type=MESH,
        )
        op.start()

    for k in (2, 3):
        for w in range(2):
            second_own(w, k)
    for w in range(2):
        second_relay(w, 0)

    shared = together(ratio_all.at[others], (ratio_send, ratio_recv))
    shared.wait_recv()
    every = ratio_all[...].astype(F32)
    rank_rows = every.shape[1] // 2
    full_ratio = []
    squares = []
    for w in range(2):
        ratio = every[:, w * rank_rows : (w + 1) * rank_rows, :].reshape(-1, every.shape[2])
        ratio_low = ratio.astype(BF16)
        full_ratio.append(ratio_low)
        high = grams[w].astype(BF16)
        rest = (grams[w] - high.astype(F32)).astype(BF16)
        spread = jnp.dot(high, ratio_low, preferred_element_type=F32)
        spread += jnp.dot(rest, ratio_low, preferred_element_type=F32)
        squares.append(jnp.sum(ratio * spread))
    lane = lax.broadcasted_iota(jnp.int32, square_out.shape, 1)
    shares = jnp.where(lane < square_out.shape[1] // 2, squares[0], squares[1])
    square_out[...] = shares
    square_in[0] = shares

    @pl.when(z < heights - 1)
    def _():
        pl.semaphore_wait(entered, 2 * (heights - 1 - z))

    for j in range(1, tp):
        op = pltpu.make_async_remote_copy(
            src_ref=square_out,
            dst_ref=square_in.at[j],
            send_sem=square_send,
            recv_sem=square_recv,
            device_id={"tp": lax.rem(tp_me + j, tp)},
            device_id_type=MESH,
        )
        op.start()

    @pl.loop(0, FS // 2)
    def _(k):
        for w in range(2):
            pair = pl.ds(pl.multiple_of(2 * rows * k, 2 * rows), 2 * rows)
            product = jnp.dot(basis[w, pair], full_ratio[w], preferred_element_type=F32)
            product = product.reshape(2, rows, product.shape[1])
            update[w, pl.ds(2 * k, 2)] = product.astype(BF16)

    for k in (1, 2):
        for w in range(2):
            second_relay(w, k)
    own_rows = pl.ds(pl.multiple_of(fs_me * rows, rows), rows)
    for w in range(2):
        own_update[w] = jnp.dot(
            basis[w, own_rows], full_ratio[w], preferred_element_type=F32
        )
    for w in range(2):
        second_relay(w, 3)

    totals = together(square_in.at[pl.ds(1, tp - 1)], (square_send, square_recv))
    totals.wait_recv()
    entries = basis.shape[1] * full_ratio[0].shape[1] * tp
    factors = lax.rsqrt(jnp.sum(square_in[...], axis=0) / entries + SCALE_FLOOR)
    scales[...] = factors

    own_share = lowered.at[:, pl.ds(0, share)]
    together(own_share, (half_send, half_recv.at[0, 0])).wait_send()
    parts.wait_send()
    shared.wait_send()
    totals.wait_send()
    for k in range(4):
        for w in range(2):
            second_last(w, k)
    for w in range(2):
        together(gathered.at[w, others], (block_send.at[w], block_recv.at[w, 0])).wait_send()


def store_kernel(
    gathered,
    update,
    own_update,
    master,
    scales,
    query_first,
    query_second,
    output_first,
    output_second,
    query_first_new,
    query_second_new,
    query_step,
    query_new,
    query_copy,
    output_first_new,
    output_second_new,
    output_step,
    output_new,
    output_copy,
    copies,
    steps,
    news,
    copy_sem,
    other_sem,
):
    fs_me = lax.axis_index("fs")
    moments = ((query_first, query_second), (output_first, output_second))
    outputs = (
        (query_first_new, query_second_new, query_step, query_new, query_copy),
        (output_first_new, output_second_new, output_step, output_new, output_copy),
    )
    half = scales.shape[1] // 2
    scale = [scales[0:1, 0:1], scales[0:1, half : half + 1]]
    rate = [(LEARN_RATE * scale[w]).astype(BF16) for w in range(2)]

    def copy_out(w, j):
        owner = lax.rem(fs_me + j, FS)
        return pltpu.make_async_copy(
            copies.at[w, owner], outputs[w][4].at[owner], copy_sem.at[w]
        )

    others = []

    def put(w, number, source):
        others.append(pltpu.make_async_copy(source, outputs[w][number], other_sem.at[w, number]))
        others[-1].start()

    @pl.loop(1, FS)
    def _(j):
        owner = lax.rem(fs_me + j, FS)
        for w in range(2):
            copies[w, owner] = gathered[w, owner] - rate[w] * update[w, owner]
            copy_out(w, j).start()

    for w in range(2):
        put(w, 0, moments[w][0])
        put(w, 1, moments[w][1])
        step = own_update[w] * scale[w]
        new = master[w] - LEARN_RATE * step
        steps[w] = step
        put(w, 2, steps.at[w])
        news[w] = new
        put(w, 3, news.at[w])
        copies[w, fs_me] = new.astype(BF16)
        copy_out(w, 0).start()

    for w in range(2):
        pltpu.make_async_copy(copies.at[w], outputs[w][4], copy_sem.at[w]).wait()
    for copy in others:
        copy.wait()


def body(
    normed,
    query_cotangent,
    attended,
    output_cotangent,
    query_basis,
    output_basis,
    query_master,
    output_master,
    query_first,
    query_second,
    output_first,
    output_second,
):
    operands = (
        normed,
        query_cotangent,
        attended,
        output_cotangent,
        query_basis,
        output_basis,
        query_master,
        output_master,
        query_first,
        query_second,
        output_first,
        output_second,
    )
    tp = lax.axis_size("tp")
    token_rows, width = normed.shape
    rank = query_basis.shape[1]
    rows, columns = query_master.shape
    rank_rows = query_first.shape[0]
    blocks, block, small = (2, FS, rows, columns), (2, rows, columns), (rank_rows, columns)
    pieces = token_rows // 2 // CHUNK
    exchanged = pl.pallas_call(
        lambda *refs: kernel(tp, *refs),
        out_shape=[
            pltpu.VMEM(blocks, BF16),
            pltpu.VMEM(blocks, BF16),
            pltpu.VMEM(block, F32),
            pltpu.VMEM(block, F32),
            pltpu.VMEM((1, 128), F32),
            pltpu.VMEM(small, F32),
            pltpu.VMEM(small, F32),
            pltpu.VMEM(small, F32),
            pltpu.VMEM(small, F32),
        ],
        in_specs=[pl.BlockSpec(memory_space=pltpu.HBM)] * 12,
        out_specs=[pl.BlockSpec(memory_space=pltpu.VMEM)] * 9,
        scratch_shapes=[
            pltpu.VMEM((2, pieces, CHUNK, width), BF16),
            pltpu.VMEM((2, width, rank), BF16),
            pltpu.VMEM((2, token_rows, columns), BF16),
            pltpu.VMEM((4, rank_rows, columns), F32),
            pltpu.VMEM((2, token_rows, 2 * rank), BF16),
            pltpu.VMEM((2, FS, rank_rows, columns), F32),
            pltpu.VMEM((FS, 2 * rank_rows, columns), BF16),
            pltpu.VMEM((FS, 2 * rank_rows, columns), BF16),
            pltpu.VMEM((FS, 2 * rank_rows, columns), BF16),
            pltpu.VMEM((1, 128), F32),
            pltpu.VMEM((tp, 1, 128), F32),
            pltpu.SemaphoreType.DMA((2,)),
            pltpu.SemaphoreType.DMA((2, 20)),
            pltpu.SemaphoreType.DMA,
            pltpu.SemaphoreType.DMA,
            pltpu.SemaphoreType.DMA,
            pltpu.SemaphoreType.DMA,
            pltpu.SemaphoreType.DMA,
            pltpu.SemaphoreType.DMA,
            pltpu.SemaphoreType.DMA,
            pltpu.SemaphoreType.DMA((2, pieces)),
            pltpu.SemaphoreType.DMA((10 + 2 * pieces,)),
            pltpu.SemaphoreType.REGULAR((3,)),
            pltpu.SemaphoreType.REGULAR,
        ],
        compiler_params=pltpu.CompilerParams(
            collective_id=0, has_side_effects=True, vmem_limit_bytes=28 * 1024 * 1024
        ),
        name="exchange",
    )(*(pltpu.with_memory_space_constraint(operand, pltpu.HBM) for operand in operands))
    per_weight = (
        jax.ShapeDtypeStruct(small, F32),
        jax.ShapeDtypeStruct(small, F32),
        jax.ShapeDtypeStruct((rows, columns), F32),
        jax.ShapeDtypeStruct((rows, columns), F32),
        jax.ShapeDtypeStruct((FS, rows, columns), BF16),
    )
    results = pl.pallas_call(
        store_kernel,
        out_shape=per_weight * 2,
        in_specs=[pl.BlockSpec(memory_space=pltpu.VMEM)] * 9,
        out_specs=[pl.BlockSpec(memory_space=pl.ANY)] * 10,
        scratch_shapes=[
            pltpu.VMEM(blocks, BF16),
            pltpu.VMEM(block, F32),
            pltpu.VMEM(block, F32),
            pltpu.SemaphoreType.DMA((2,)),
            pltpu.SemaphoreType.DMA((2, 4)),
        ],
        compiler_params=pltpu.CompilerParams(vmem_limit_bytes=16 * 1024 * 1024),
        name="store",
    )(*exchanged)
    return tuple(r.reshape(-1, columns) for r in results)


def solution(mesh):
    in_specs = (
        P("fs", None),
        P("fs", "tp"),
        P("fs", "tp"),
        P("fs", None),
        P(),
        P(),
        P("fs", "tp"),
        P("fs", "tp"),
        P("fs", "tp"),
        P("fs", "tp"),
        P("fs", "tp"),
        P("fs", "tp"),
    )
    out_specs = (
        P("fs", "tp"),
        P("fs", "tp"),
        P("fs", "tp"),
        P("fs", "tp"),
        P(None, "tp"),
        P("fs", "tp"),
        P("fs", "tp"),
        P("fs", "tp"),
        P("fs", "tp"),
        P(None, "tp"),
    )
    return jax.shard_map(body, mesh=mesh, in_specs=in_specs, out_specs=out_specs, check_vma=False)
```

time: 38.8 us -> 36.3 us (0.936)
  Pallas kernels: 38.1 us -> 35.5 us
    pallas_call x2, Pallas kernels: 38.1 us -> 35.5 us  [the longest x1 32.6 us: body(): pl.pallas_call(lambda *refs: kernel(tp, *refs), out_shape=[pltpu.VMEM(blo...]
where the time goes in v3:
time: 36.3 us; the launch traced here: 36.2 us
  Pallas kernels  35.5 us (98%)
  between operations  0.66 us (2%)
    pallas_call x1, Pallas kernels, body(): pl.pallas_call(lambda *refs: kernel(tp, *refs), out_shape=[pltpu.VMEM(blo...  32.6 us
    pallas_call x1, Pallas kernels, body(): pl.pallas_call(store_kernel, out_shape=per_weight * 2, in_specs=[pl.Block...  2.96 us

profile of v3, /device:TPU:1, one launch (start us, length us, event | category | flops | bytes accessed | tf_op | source)
XLA Modules:
  0.0 36.2 jit_solution(16860051497649857683)
XLA Ops:
  0.6 32.6 %exchange.1 = (bf16[2,16,256,256]{3,2,1,0:T(8,128)(2,1)S(1)}, bf16[2,16,256,256]{3,2,1,0:T(8,128)(2,1)S(1)}, f32[2,256,256]{2,1,0:T(8,128)S(1)}, f32[2,256,256]{...) custom-call(bf16[1024,4096]{1,0:T(8,128)(2,1)} %refs_0_.1, ...), custom_call_target="tpu_custom_call" | custom-call | tf_op jit(solution)/shard_map/exchange/pallas_call | solution.py:522
  33.2 3.0 %store.1 = (f32[8,256]{1,0:T(8,128)}, f32[8,256]{1,0:T(8,128)}, f32[256,256]{1,0:T(8,128)}, f32[256,256]{1,0:T(8,128)}, bf16[16,256,256]{2,1,0:T(8,128)(2,1)}, /...) custom-call(bf16[2,16,256,256]{3,2,1,0:T(8,128)(2,1)S(1)} %get-tuple, ...), custom_call_target="tpu_custom_call" | custom-call | tf_op jit(solution)/shard_map/store/pallas_call | solution.py:575

commit v4 on v3

--- a/solution.py
+++ b/solution.py
@@ -17,7 +17,7 @@
 SIDE = 4
 FS = SIDE * SIDE
 CHUNK = 128
-UPPER = 128
+UPPER = 112
 STEPS = (0, -1, 1, 2)
 
 
@@ -91,16 +91,6 @@
         for device in near:
             tell(sem, device)
 
-    barrier = pltpu.get_barrier_semaphore()
-    greet(barrier)
-    tell(barrier, partner)
-    for dz in range(1, heights):
-
-        @pl.when(z + dz < heights)
-        def _():
-            for c in range(2):
-                tell(barrier, {"tp": (z + dz) * 2 + c})
-
     sources = (normed, output_cotangent)
     share = normed.shape[0] // 2
     chunks = share // CHUNK
@@ -130,7 +120,21 @@
     loads = []
     for k, (src, dst) in enumerate(pieces):
         loads.append(pltpu.make_async_copy(src, dst, local_sem.at[k]))
-        loads[-1].start()
+    for load in loads[:2]:
+        load.start()
+
+    barrier = pltpu.get_barrier_semaphore()
+    greet(barrier)
+    tell(barrier, partner)
+    for dz in range(1, heights):
+
+        @pl.when(z + dz < heights)
+        def _():
+            for c in range(2):
+                tell(barrier, {"tp": (z + dz) * 2 + c})
+
+    for load in loads[2:]:
+        load.start()
 
     for w in range(2):
         loads[w].wait()
@@ -437,7 +441,6 @@
     copy_sem,
     other_sem,
 ):
-    fs_me = lax.axis_index("fs")
     moments = ((query_first, query_second), (output_first, output_second))
     outputs = (
         (query_first_new, query_second_new, query_step, query_new, query_copy),
@@ -447,40 +450,33 @@
     scale = [scales[0:1, 0:1], scales[0:1, half : half + 1]]
     rate = [(LEARN_RATE * scale[w]).astype(BF16) for w in range(2)]
 
-    def copy_out(w, j):
-        owner = lax.rem(fs_me + j, FS)
-        return pltpu.make_async_copy(
-            copies.at[w, owner], outputs[w][4].at[owner], copy_sem.at[w]
-        )
-
-    others = []
+    copying = []
 
     def put(w, number, source):
-        others.append(pltpu.make_async_copy(source, outputs[w][number], other_sem.at[w, number]))
-        others[-1].start()
-
-    @pl.loop(1, FS)
-    def _(j):
-        owner = lax.rem(fs_me + j, FS)
+        copying.append(
+            pltpu.make_async_copy(source, outputs[w][number], other_sem.at[w, number])
+        )
+        copying[-1].start()
+
+    for owner in range(FS):
         for w in range(2):
             copies[w, owner] = gathered[w, owner] - rate[w] * update[w, owner]
-            copy_out(w, j).start()
+            pltpu.make_async_copy(
+                copies.at[w, owner], outputs[w][4].at[owner], copy_sem.at[w]
+            ).start()
 
     for w in range(2):
         put(w, 0, moments[w][0])
         put(w, 1, moments[w][1])
         step = own_update[w] * scale[w]
-        new = master[w] - LEARN_RATE * step
         steps[w] = step
         put(w, 2, steps.at[w])
-        news[w] = new
+        news[w] = master[w] - LEARN_RATE * step
         put(w, 3, news.at[w])
-        copies[w, fs_me] = new.astype(BF16)
-        copy_out(w, 0).start()
 
     for w in range(2):
         pltpu.make_async_copy(copies.at[w], outputs[w][4], copy_sem.at[w]).wait()
-    for copy in others:
+    for copy in copying:
         copy.wait()
 
 

time: 36.3 us -> 35.2 us (0.970)
  Pallas kernels: 35.5 us -> 34.5 us
    pallas_call x1, Pallas kernels: 32.6 us -> 32 us  [body(): pl.pallas_call(lambda *refs: kernel(tp, *refs), out_shape=[pltpu.VMEM(blo...]
    pallas_call x1, Pallas kernels: 2.96 us -> 2.49 us  [body(): pl.pallas_call(store_kernel, out_shape=per_weight * 2, in_specs=[pl.Block...]
where the time goes in v4:
time: 35.2 us; the launch traced here: 35.1 us
  Pallas kernels  34.5 us (98%)
  between operations  0.66 us (2%)
    pallas_call x1, Pallas kernels, body(): pl.pallas_call(lambda *refs: kernel(tp, *refs), out_shape=[pltpu.VMEM(blo...  32 us
    pallas_call x1, Pallas kernels, body(): pl.pallas_call(store_kernel, out_shape=per_weight * 2, in_specs=[pl.Block...  2.49 us

profile of v4, /device:TPU:1, one launch (start us, length us, event | category | flops | bytes accessed | tf_op | source)
XLA Modules:
  0.0 35.1 jit_solution(12049370122379824692)
XLA Ops:
  0.6 32.0 %exchange.1 = (bf16[2,16,256,256]{3,2,1,0:T(8,128)(2,1)S(1)}, bf16[2,16,256,256]{3,2,1,0:T(8,128)(2,1)S(1)}, f32[2,256,256]{2,1,0:T(8,128)S(1)}, f32[2,256,256]{...) custom-call(bf16[1024,4096]{1,0:T(8,128)(2,1)} %refs_0_.1, ...), custom_call_target="tpu_custom_call" | custom-call | tf_op jit(solution)/shard_map/exchange/pallas_call | solution.py:518
  32.6 2.5 %store.1 = (f32[8,256]{1,0:T(8,128)}, f32[8,256]{1,0:T(8,128)}, f32[256,256]{1,0:T(8,128)}, f32[256,256]{1,0:T(8,128)}, bf16[16,256,256]{2,1,0:T(8,128)(2,1)}, /...) custom-call(bf16[2,16,256,256]{3,2,1,0:T(8,128)(2,1)S(1)} %get-tuple, ...), custom_call_target="tpu_custom_call" | custom-call | tf_op jit(solution)/shard_map/store/pallas_call | solution.py:571

commit v5 on v4

--- a/solution.py
+++ b/solution.py
@@ -16,9 +16,19 @@
 
 SIDE = 4
 FS = SIDE * SIDE
-CHUNK = 128
+CHUNK = 256
 UPPER = 112
 STEPS = (0, -1, 1, 2)
+
+
+def hops(offset, size):
+    return min(offset, size - offset)
+
+
+OTHERS = sorted(
+    ((dy, dx) for dy in range(SIDE) for dx in range(SIDE) if dy or dx),
+    key=lambda o: -hops(o[0], SIDE) - hops(o[1], SIDE),
+)
 
 
 def kernel(
@@ -263,7 +273,7 @@
             if w == 1 and k == 0:
                 next_round(0)
                 finish(0)
-            if w == 1 and k == 2:
+            if w == 1 and k == chunks - 1:
                 next_round(1)
         first += chunks
     loads[first].wait()
@@ -272,11 +282,11 @@
     partial_out[...] = jnp.concatenate([partial[0], partial[1]], axis=1).astype(BF16)
     next_round(2)
 
-    for j in range(1, FS):
-        target = lax.rem(fs_me + j, FS)
+    for dy, dx in OTHERS:
+        target = at(dy, dx)
         op = pltpu.make_async_remote_copy(
             src_ref=partial_out.at[target],
-            dst_ref=partial_in.at[j],
+            dst_ref=partial_in.at[dy * SIDE + dx],
             send_sem=part_send,
             recv_sem=part_recv,
             device_id={"fs": target},
@@ -326,13 +336,13 @@
         ratios.append(first_new / jnp.sqrt(second_new + SECOND_FLOOR))
     ratio_all[fs_me] = jnp.concatenate(ratios, axis=0).astype(BF16)
 
-    for j in range(1, FS):
+    for dy, dx in OTHERS:
         op = pltpu.make_async_remote_copy(
             src_ref=ratio_all.at[fs_me],
             dst_ref=ratio_all.at[fs_me],
             send_sem=ratio_send,
             recv_sem=ratio_recv,
-            device_id={"fs": lax.rem(fs_me + j, FS)},
+            device_id={"fs": at(dy, dx)},
             device_id_type=MESH,
         )
         op.start()
@@ -367,13 +377,17 @@
     def _():
         pl.semaphore_wait(entered, 2 * (heights - 1 - z))
 
-    for j in range(1, tp):
+    peers = sorted(
+        ((dz, c) for dz in range(heights) for c in range(2) if dz or c),
+        key=lambda o: -hops(o[0], heights),
+    )
+    for dz, c in peers:
         op = pltpu.make_async_remote_copy(
             src_ref=square_out,
-            dst_ref=square_in.at[j],
+            dst_ref=square_in.at[2 * dz + c],
             send_sem=square_send,
             recv_sem=square_recv,
-            device_id={"tp": lax.rem(tp_me + j, tp)},
+            device_id={"tp": ((z + dz) % heights) * 2 + (core + c) % 2},
             device_id_type=MESH,
         )
         op.start()

time: 35.2 us -> 34.6 us (0.983)
  Pallas kernels: 34.5 us -> 33.9 us
    pallas_call x1, Pallas kernels: 32 us -> 31.4 us  [body(): pl.pallas_call(lambda *refs: kernel(tp, *refs), out_shape=[pltpu.VMEM(blo...]
where the time goes in v5:
time: 34.6 us; the launch traced here: 34.5 us
  Pallas kernels  33.9 us (98%)
  between operations  0.66 us (2%)
    pallas_call x1, Pallas kernels, body(): pl.pallas_call(lambda *refs: kernel(tp, *refs), out_shape=[pltpu.VMEM(blo...  31.4 us
    pallas_call x1, Pallas kernels, body(): pl.pallas_call(store_kernel, out_shape=per_weight * 2, in_specs=[pl.Block...  2.49 us

profile of v5, /device:TPU:1, one launch (start us, length us, event | category | flops | bytes accessed | tf_op | source)
XLA Modules:
  0.0 34.5 jit_solution(16163451792603849978)
XLA Ops:
  0.6 31.4 %exchange.1 = (bf16[2,16,256,256]{3,2,1,0:T(8,128)(2,1)S(1)}, bf16[2,16,256,256]{3,2,1,0:T(8,128)(2,1)S(1)}, f32[2,256,256]{2,1,0:T(8,128)S(1)}, f32[2,256,256]{...) custom-call(bf16[1024,4096]{1,0:T(8,128)(2,1)} %refs_0_.1, ...), custom_call_target="tpu_custom_call" | custom-call | tf_op jit(solution)/shard_map/exchange/pallas_call | solution.py:532
  32.1 2.5 %store.1 = (f32[8,256]{1,0:T(8,128)}, f32[8,256]{1,0:T(8,128)}, f32[256,256]{1,0:T(8,128)}, f32[256,256]{1,0:T(8,128)}, bf16[16,256,256]{2,1,0:T(8,128)(2,1)}, /...) custom-call(bf16[2,16,256,256]{3,2,1,0:T(8,128)(2,1)S(1)} %get-tuple, ...), custom_call_target="tpu_custom_call" | custom-call | tf_op jit(solution)/shard_map/store/pallas_call | solution.py:585
